TPU v7x, 512 devices: a whole 4x8x8 slice. The times are simulated.
512 devices in a mesh: sp: 64 (over z, y), tp: 8 (over x, core).
Axes of the slice: x: 4, y: 8, z: 8, core: 2. Of those that a mesh axis runs over, the one named last changes fastest.
Arguments:
- residual: bfloat16 [8192, 2048], P(('sp', 'tp')), may hold values from -6 to 6
- q_small: bfloat16 [8192, 1024], P('sp', 'tp'), may hold values from -6 to 6
- k_small: bfloat16 [8192, 1024], P('sp', 'tp'), may hold values from -6 to 6
- v_small: bfloat16 [8192, 1024], P('sp', 'tp'), may hold values from -6 to 6
- q_large: bfloat16 [8192, 1024], P('sp', 'tp'), may hold values from -6 to 6
- k_large: bfloat16 [8192, 1024], P('sp', 'tp'), may hold values from -6 to 6
- v_large: bfloat16 [8192, 1024], P('sp', 'tp'), may hold values from -6 to 6
- forget_small: float32 [8192, 16], P('sp', 'tp'), may hold values from 0 to 20
- forget_large: float32 [8192, 8], P('sp', 'tp'), may hold values from 0 to 20
- w_out_small: bfloat16 [1024, 2048], P('tp'), may hold values from -0.125 to 0.125
- w_out_large: bfloat16 [1024, 2048], P('tp'), may hold values from -0.125 to 0.125
- norm_gain: float32 [2048], replicated, may hold values from 0.1 to 1.9
- w_gate: bfloat16 [2048, 4096], P('sp', 'tp'), may hold values from -0.125 to 0.125
- w_up: bfloat16 [2048, 4096], P('sp', 'tp'), may hold values from -0.125 to 0.125
- conv_gate: float32 [3, 4096], P(None, 'tp'), may hold values from -3 to 3
- conv_up: float32 [3, 4096], P(None, 'tp'), may hold values from -3 to 3
- w_down: bfloat16 [4096, 2048], P('tp', 'sp'), may hold values from -0.09375 to 0.09375
Outputs:
- mixed: bfloat16 [8192, 2048], P(('sp', 'tp'))
All inputs are finite; a program needn't handle non-finite values.
Results may differ from a plain program's by a relative error of at most 0.015.
Values may be sent and summed in bfloat16 or wider, within the bound.
A program may use at most 64 MiB of HBM per device.

v0:
```python
import jax
import jax.numpy as jnp
from jax import lax
from jax.sharding import PartitionSpec as P

EPS = 1e-06
NEG = -1e30


def rows_first(arrays, axis, dims):
    turned = [jnp.moveaxis(a, dim, 0) for a, dim in zip(arrays, dims)]
    widths = [t[0].size for t in turned]
    both = jnp.concatenate([t.reshape(-1, w) for t, w in zip(turned, widths)], axis=1)
    whole = lax.all_gather(both, axis, axis=0, tiled=True)
    parts = jnp.split(whole, [sum(widths[:k]) for k in range(1, len(widths))], axis=1)
    return tuple(
        (
            jnp.moveaxis(b.reshape(-1, *t.shape[1:]), 0, dim)
            for b, t, dim in zip(parts, turned, dims)
        )
    )


def in_one_piece(arrays, axis, dim, along):
    widths = [a.shape[along] for a in arrays]
    both = jnp.concatenate(arrays, axis=along)
    whole = lax.all_gather(both, axis, axis=dim, tiled=True)
    return tuple(jnp.split(whole, [sum(widths[:k]) for k in range(1, len(widths))], axis=along))


def in_blocks(array, dim, size):
    before, after = (array.shape[:dim], array.shape[dim + 1 :])
    return jnp.moveaxis(array.reshape(*before, size, -1, *after), dim, 0)


def sent_and_summed(array, axis, dim):
    size = lax.axis_size(axis)
    parts = lax.all_to_all(in_blocks(array, dim, size), axis, 0, 0, tiled=True)
    return jnp.sum(parts.astype(jnp.float32), axis=0)


def sent_to_all(array, axis):
    size = lax.axis_size(axis)
    return lax.all_to_all(
        jnp.broadcast_to(array[None], (size, *array.shape)), axis, 0, 0, tiled=True
    )


def in_order(parts, dim):
    parts = jnp.moveaxis(parts, 0, dim)
    lengths = parts.shape
    return parts.reshape(*lengths[:dim], lengths[dim] * lengths[dim + 1], *lengths[dim + 2 :])


def gather_directly(array, axis, dim):
    parts = sent_to_all(array, axis)
    return in_order(parts, dim)


def from_behind(block, axis, distance):
    devices = range(lax.axis_size(axis))
    route = [(i - distance, i) for i in devices if i - distance in devices]
    return lax.ppermute(block, axis, route)


def globalize(part, rows):
    heads = part.shape[1]
    blocks = part.reshape(-1, rows, heads)
    totals = blocks[:, -1, :]
    before = jnp.cumsum(totals, axis=0) - totals
    return (blocks + before[:, None, :]).reshape(part.shape)


def attend(carry, keys, values, queries, cum_own, cum_every, qpos):
    top, denom, accum = carry
    count = keys.shape[0]
    heads = queries.shape[1]
    size = queries.shape[2]
    keys = keys.reshape(count, heads, size)
    values = values.reshape(count, heads, size)
    kpos = jnp.arange(count, dtype=jnp.int32)
    scores = jnp.einsum(
        "qhd,khd->qhk", queries, keys, preferred_element_type=jnp.float32
    ) * size ** (-0.5)
    scores = scores + cum_own[:, :, None] - cum_every.T[None, :, :]
    keep = (kpos[None, :] <= qpos[:, None])[:, None, :]
    scores = jnp.where(keep, scores, NEG)
    new_top = jnp.maximum(top, jnp.max(scores, axis=-1))
    weights = jnp.where(keep, jnp.exp(scores - new_top[:, :, None]), 0.0)
    denom = jnp.sum(weights, axis=-1)
    accum = jnp.einsum(
        "qhk,khd->qhd", weights.astype(jnp.bfloat16), values, preferred_element_type=jnp.float32
    )
    return (new_top, denom, accum)


def finish(carry):
    top, denom, accum = carry
    attended = accum / denom[:, :, None]
    normed = attended * lax.rsqrt(jnp.mean(attended * attended, axis=-1, keepdims=True) + EPS)
    return normed.astype(jnp.bfloat16).reshape(attended.shape[0], -1)


def empty_carry(rows, heads, size):
    return (
        jnp.full((rows, heads), NEG, jnp.float32),
        jnp.zeros((rows, heads), jnp.float32),
        jnp.zeros((rows, heads, size), jnp.float32),
    )


def body(
    residual,
    q_small,
    k_small,
    v_small,
    q_large,
    k_large,
    v_large,
    forget_small,
    forget_large,
    w_out_small,
    w_out_large,
    norm_gain,
    w_gate,
    w_up,
    conv_gate,
    conv_up,
    w_down,
):
    rows = q_small.shape[0]
    offset = lax.axis_index("sp") * rows
    qpos = offset + jnp.arange(rows, dtype=jnp.int32)
    gathered = rows_first((w_gate, w_up, w_down), "sp", (0, 0, 1))
    local_small = jnp.cumsum(jax.nn.log_sigmoid(forget_small), axis=0)
    local_large = jnp.cumsum(jax.nn.log_sigmoid(forget_large), axis=0)
    part_small, part_large = in_one_piece((local_small, local_large), "sp", 0, 1)
    every_small = globalize(part_small, rows)
    every_large = globalize(part_large, rows)
    cum_small = lax.dynamic_slice_in_dim(every_small, offset, rows, 0)
    cum_large = lax.dynamic_slice_in_dim(every_large, offset, rows, 0)
    heads_small = forget_small.shape[1]
    heads_large = forget_large.shape[1]
    queries_small = q_small.reshape(rows, heads_small, -1)
    queries_large = q_large.reshape(rows, heads_large, -1)
    start_carry = (
        empty_carry(rows, heads_small, queries_small.shape[2]),
        empty_carry(rows, heads_large, queries_large.shape[2]),
    )
    keys_s, values_s, keys_l, values_l = in_one_piece(
        (k_small, v_small, k_large, v_large), "sp", 0, 1
    )
    small = attend(start_carry[0], keys_s, values_s, queries_small, cum_small, every_small, qpos)
    large = attend(start_carry[1], keys_l, values_l, queries_large, cum_large, every_large, qpos)
    normed_small = finish(small)
    normed_large = finish(large)
    first_part = jnp.dot(normed_small, w_out_small, preferred_element_type=jnp.float32)
    projected = sent_and_summed(
        (
            first_part + jnp.dot(normed_large, w_out_large, preferred_element_type=jnp.float32)
        ).astype(jnp.bfloat16),
        "tp",
        0,
    )
    first = residual.astype(jnp.float32) + projected
    normal = (
        first * lax.rsqrt(jnp.mean(first * first, axis=-1, keepdims=True) + EPS) * norm_gain
    ).astype(jnp.bfloat16)
    gate_full, up_full, down_full = gathered
    piece = gather_directly(normal, "tp", 0)
    gate_part = jnp.dot(piece, gate_full, preferred_element_type=jnp.float32).astype(jnp.bfloat16)
    up_part = jnp.dot(piece, up_full, preferred_element_type=jnp.float32).astype(jnp.bfloat16)
    both = jnp.concatenate([gate_part, up_part], axis=1)
    width = both.shape[0]
    rim = from_behind(both[width - 2 :], "sp", 1)
    extended = jnp.concatenate([rim, both], axis=0).astype(jnp.float32)
    taps = jnp.concatenate([conv_gate, conv_up], axis=1)
    conv = (
        taps[0] * extended[0:width]
        + taps[1] * extended[1 : width + 1]
        + taps[2] * extended[2 : width + 2]
    )
    half = gate_full.shape[1]
    hidden = (jax.nn.silu(conv[:, :half]) * conv[:, half:]).astype(jnp.bfloat16)
    mixed = first + sent_and_summed(
        jnp.dot(hidden, down_full, preferred_element_type=jnp.float32).astype(jnp.bfloat16), "tp", 0
    )
    return mixed.astype(jnp.bfloat16)


def solution(mesh):
    placed = (
        P(("sp", "tp"), None),
        P("sp", "tp"),
        P("sp", "tp"),
        P("sp", "tp"),
        P("sp", "tp"),
        P("sp", "tp"),
        P("sp", "tp"),
        P("sp", "tp"),
        P("sp", "tp"),
        P("tp", None),
        P("tp", None),
        P(),
        P("sp", "tp"),
        P("sp", "tp"),
        P(None, "tp"),
        P(None, "tp"),
        P("tp", "sp"),
    )
    return jax.shard_map(
        body, mesh=mesh, in_specs=placed, out_specs=P(("sp", "tp"), None), check_vma=False
    )
```

profile of v0, /device:TPU:64, one launch (start us, length us, event | category | flops | bytes accessed | tf_op | source)
XLA Modules:
  0.0 240.2 jit_solution(16217018536142575278)
XLA Ops:
  6.5 1.5 pad_maximum_fusion
  8.2 1.4 pad_maximum_fusion.1
  9.6 0.7 fusion.63
  10.7 0.7 fusion.66
  11.7 54.8 %all_gather.10 = f32[8192,3]{0,1:T(4,128)S(1)} all-gather(f32[128,3]{0,1:T(4,128)S(1)} %pad_maximum_fusion.3), channel_id=1, replica_groups=mesh['sp'=64,'tp'=8] {'sp'}, dimensions={0}, use_global_device_ids=true | all-gather | bytes 99840 | tf_op jit(solution)/shard_map/all_gather | solution.py:27
  66.7 0.6 fusion.73
  67.3 2.7 %copy.48 = f32[8192,2]{1,0:T(8,128)} copy(f32[8192,2]{0,1:T(2,128)S(1)} %split.38) | data formatting | bytes 131072 | tf_op jit(solution)/shard_map/split | solution.py:28
  70.0 1.3 reduce-window_subtract_fusion.1
  71.8 1.7 iota_compare_fusion.1
  73.5 38.8 %all-gather.3.cloned.1.call-done = bf16[8192,512]{1,0:T(8,128)(2,1)} async-done(((bf16[128,512]{1,0:T(8,128)(2,1)}), bf16[8192,512]{1,0:T(8,128)(2,1)}) %all-gather.3.cloned.1.call-update) | async-done | bytes 8388624 | tf_op jit(solution)/shard_map/all_gather | solution.py:27
  112.3 3.9 %fusion.70 = (bf16[8192,128]{1,0:T(8,128)(2,1)}, bf16[8192,128]{1,0:T(8,128)(2,1)S(1)}) fusion(bf16[8192,512]{1,0:T(8,128)(2,1)} %all-gather.3.cloned.1.call-done), kind=kLoop, calls=%fused_computation.95 | loop fusion | bytes 8388608 | tf_op jit(solution)/shard_map/split | solution.py:28
  116.2 4.1 %copy.42 = bf16[8192,128]{0,1:T(8,128)(2,1)} copy(bf16[8192,128]{1,0:T(8,128)(2,1)} %get-tuple-element.5) | data formatting | bytes 4194304 | tf_op jit(solution)/shard_map/split | solution.py:28
  120.2 2.9 %copy.41 = bf16[8192,128]{0,1:T(8,128)(2,1)} copy(bf16[8192,128]{1,0:T(8,128)(2,1)S(1)} %get-tuple-element.6) | data formatting | bytes 4194304 | tf_op jit(solution)/shard_map/split | solution.py:28
  123.2 3.5 %fusion.74 = (f32[128]{0:T(128)S(1)}, f32[128,1,8192]{0,2,1:T(8,128)S(1)}) fusion(f32[8192]{0:T(1024)S(1)} %bitcast_add_fusion.1, f32[128]{0:T(128)S(1)} %fusion.65, bf16[128,128]{1,0:T(8,128)(2,1)S(1)} %copy-done.10, bf16[8192,512]{1,0:T(8,128)(2,1)} %all-gather.3.cloned.1.call-done, s32[128]{0:T(128)S(1)} %iota_add_fusion), kind=kOutput, calls=%fused_computation.99 | convolution fusion | flops 274726784 | bytes 6358528 | tf_op jit(solution)/shard_map/qhd,khd->qhk/dot_general | solution.py:82
  126.7 1.1 fusion.16
  127.9 2.9 %multiply_reduce_fusion.1 = (f32[128]{0:T(128)S(1)}, f32[1,128,128]{2,1,0:T(8,128)S(1)}) fusion(f32[128]{0:T(128)S(1)} %fusion.16, f32[128,1,8192]{0,2,1:T(8,128)S(1)} %get-tuple-element.15, f32[128]{0:T(128)S(1)} %broadcast_maximum_fusion.1, s32[128]{0:T(128)S(1)} %iota_add_fusion, bf16[8192,512]{1,0:T(8,128)(2,1)} %all-gather.3.cloned.1.call-done), kind=kOutput, calls=%fused_computation.65 | convolution fusion | flops 272678784 | bytes 6359040 | tf_op jit(solution)/shard_map/qhk,khd->qhd/dot_general | solution.py:91
  130.8 3.6 %fusion.72 = (f32[128,2]{0,1:T(2,128)S(1)}, f32[128,2,8192]{0,2,1:T(8,128)S(1)}) fusion(f32[2,8192]{1,0:T(2,128)S(1)} %bitcast.93, f32[128,2]{0,1:T(2,128)S(1)} %constant_dynamic-slice_fusion.2, bf16[8192,2,64]{0,2,1:T(8,128)(2,1)S(1)} %bitcast.85, bf16[128,2,64]{0,2,1:T(8,128)(2,1)S(1)} %bitcast.95, pred[128,8192]{0,1:T(8,128)(4,1)S(1)} %copy-done.1), kind=kOutput, calls=%fused_computation.97 | convolution fusion | flops 278920960 | bytes 11634688 | tf_op jit(solution)/shard_map/qhd,khd->qhk/dot_general | solution.py:82
  134.5 1.7 fusion.9
  136.2 2.1 multiply_reduce_fusion.2
  138.4 0.3 fusion.75
  138.8 0.3 fusion.18
  139.1 14.4 %all_to_all.15 = bf16[8,16,2048]{2,1,0:T(8,128)(2,1)S(1)} all-to-all(bf16[8,16,2048]{2,1,0:T(8,128)(2,1)S(1)} %bitcast.83), channel_id=1, replica_groups=mesh['sp'=64,'tp'=8] {'tp'}, dimensions={0} | all-to-all | bytes 1048576 | tf_op jit(solution)/shard_map/all_to_all | solution.py:38
  153.8 0.8 broadcast_in_dim.63
  154.7 3.5 %all-to-all-start.1 = ((bf16[8,16,2048]{2,1,0:T(8,128)(2,1)}), bf16[8,16,2048]{2,1,0:T(8,128)(2,1)S(1)}, u32[]{:S(2)}, u32[]{:S(2)}) async-start(bf16[8,16,2048]{2,1,0:T(8,128)(2,1)} %broadcast_in_dim.63), calls=%async_computation.1 | async-start | bytes 1048576 | tf_op jit(solution)/shard_map/all_to_all | solution.py:44
  158.2 45.6 %all-gather.5.cloned.1.call-done = bf16[2048,1536]{1,0:T(8,128)(2,1)} async-done(((bf16[32,1536]{1,0:T(8,128)(2,1)}), bf16[2048,1536]{1,0:T(8,128)(2,1)}) %all-gather.5.cloned.1.call-update) | async-done | bytes 6291472 | tf_op jit(solution)/shard_map/all_gather | solution.py:14
  203.9 2.0 fusion.32
  205.9 2.0 fusion.35
  208.0 3.1 %collective-permute-start = (bf16[2,1024]{1,0:T(2,128)(2,1)S(1)}, bf16[2,1024]{1,0:T(2,128)(2,1)S(1)}, u32[]{:S(2)}, u32[]{:S(2)}) collective-permute-start(bf16[2,1024]{1,0:T(2,128)(2,1)S(1)} %pad_maximum_fusion.2), channel_id=1, source_target_pairs={{0,8},{8,16},{16,24},{24,32},{32,40},{40,48},{48,56},{56,64},{64,7... | collective-permute-start | bytes 12296 | tf_op jit(solution)/shard_map/ppermute | solution.py:63
  211.0 4.5 %collective-permute-done = bf16[2,1024]{1,0:T(2,128)(2,1)S(1)} collective-permute-done((bf16[2,1024]{1,0:T(2,128)(2,1)S(1)}, bf16[2,1024]{1,0:T(2,128)(2,1)S(1)}, u32[]{:S(2)}, u32[]{:S(2)}) %collective-permute-start) | collective-permute-done | bytes 4128 | tf_op jit(solution)/shard_map/ppermute | solution.py:63
  215.8 2.4 %convolution_convert_fusion = bf16[128,2048]{1,0:T(8,128)(2,1)S(1)} fusion(bf16[2048,1536]{1,0:T(8,128)(2,1)} %all-gather.5.cloned.1.call-done, f32[128,1024]{1,0:T(8,128)S(1)} %fusion.54), kind=kOutput, calls=%fused_computation.25 | convolution fusion | flops 269090816 | bytes 3145728 | tf_op jit(solution)/shard_map/dot_general | solution.py:186
  218.2 14.4 %all_to_all.16 = bf16[8,16,2048]{2,1,0:T(8,128)(2,1)S(1)} all-to-all(bf16[8,16,2048]{2,1,0:T(8,128)(2,1)S(1)} %bitcast.88), channel_id=1, replica_groups=mesh['sp'=64,'tp'=8] {'tp'}, dimensions={0} | all-to-all | bytes 1048576 | tf_op jit(solution)/shard_map/all_to_all | solution.py:38
  232.7 0.7 add_convert_fusion
  (62 shorter events, 2.2 us)
Async XLA Ops:
  6.5 131.9 %copy-start = (bf16[128,2048]{1,0:T(8,128)(2,1)S(1)}, bf16[128,2048]{1,0:T(8,128)(2,1)}, u32[]{:S(2)}) copy-start(bf16[128,2048]{1,0:T(8,128)(2,1)} %param.26) | copy-start | bytes 1572868
  6.5 64.9 %copy-start.6 = (bf16[128,128]{1,0:T(8,128)(2,1)S(1)}, bf16[128,128]{1,0:T(8,128)(2,1)}, u32[]{:S(2)}) copy-start(bf16[128,128]{1,0:T(8,128)(2,1)} %param.18) | copy-start | bytes 98308
  6.5 105.8 %all-gather.3.cloned.1.call-start = ((), (), s32[]{:S(2)}) async-start(), calls=%async_computation.3 | async-start | bytes 8519680 | tf_op jit(solution)/shard_map/all_gather | solution.py:27
  8.1 195.8 %all-gather.5.cloned.1.call-start = ((), (), s32[]{:S(2)}) async-start(), calls=%async_computation.4 | async-start | bytes 6389760 | tf_op jit(solution)/shard_map/all_gather | solution.py:14
  116.2 7.0 %copy-start.10 = (bf16[128,128]{1,0:T(8,128)(2,1)S(1)}, bf16[128,128]{1,0:T(8,128)(2,1)}, u32[]{:S(2)}) copy-start(bf16[128,128]{1,0:T(8,128)(2,1)} %param.21) | copy-start | bytes 98308
  127.8 3.0 %copy-start.1 = (pred[128,8192]{0,1:T(8,128)(4,1)S(1)}, pred[128,8192]{0,1:T(8,128)(4,1)}, u32[]{:S(2)}) copy-start(pred[128,8192]{0,1:T(8,128)(4,1)} %iota_compare_fusion.1) | copy-start | bytes 3145732
  127.8 3.0 %copy-start.3 = (bf16[8192,128]{0,1:T(8,128)(2,1)S(1)}, bf16[8192,128]{0,1:T(8,128)(2,1)}, u32[]{:S(2)}) copy-start(bf16[8192,128]{0,1:T(8,128)(2,1)} %copy.42) | copy-start | bytes 6291460
  134.5 1.7 copy-start.2
  136.2 2.6 %copy-start.5 = (bf16[128,2048]{1,0:T(8,128)(2,1)S(1)}, bf16[128,2048]{1,0:T(8,128)(2,1)}, u32[]{:S(2)}) copy-start(bf16[128,2048]{1,0:T(8,128)(2,1)} %param.27) | copy-start | bytes 1572868
  138.3 15.2 %copy-start.4 = (bf16[16,2048]{1,0:T(8,128)(2,1)S(1)}, bf16[16,2048]{1,0:T(8,128)(2,1)}, u32[]{:S(2)}) copy-start(bf16[16,2048]{1,0:T(8,128)(2,1)} %param.17) | copy-start | bytes 196612
  138.3 15.4 %copy-start.7 = (f32[2048]{0:T(1024)S(1)}, f32[2048]{0:T(1024)}, u32[]{:S(2)}) copy-start(f32[2048]{0:T(1024)} %param.28) | copy-start | bytes 24580
  138.4 19.8 %copy-start.8 = (f32[3,512]{1,0:T(4,128)S(1)}, f32[3,512]{1,0:T(4,128)}, u32[]{:S(2)}) copy-start(f32[3,512]{1,0:T(4,128)} %param.31) | copy-start | bytes 18436
  138.4 19.8 %copy-start.9 = (f32[3,512]{1,0:T(4,128)S(1)}, f32[3,512]{1,0:T(4,128)}, u32[]{:S(2)}) copy-start(f32[3,512]{1,0:T(4,128)} %param.32) | copy-start | bytes 18436
  154.7 49.2 %all-to-all-start.1 = ((bf16[8,16,2048]{2,1,0:T(8,128)(2,1)}), bf16[8,16,2048]{2,1,0:T(8,128)(2,1)S(1)}, u32[]{:S(2)}, u32[]{:S(2)}) async-start(bf16[8,16,2048]{2,1,0:T(8,128)(2,1)} %broadcast_in_dim.63), calls=%async_computation.1 | async-start | bytes 1048576 | tf_op jit(solution)/shard_map/all_to_all | solution.py:44
  208.0 7.6 %collective-permute-start = (bf16[2,1024]{1,0:T(2,128)(2,1)S(1)}, bf16[2,1024]{1,0:T(2,128)(2,1)S(1)}, u32[]{:S(2)}, u32[]{:S(2)}) collective-permute-start(bf16[2,1024]{1,0:T(2,128)(2,1)S(1)} %pad_maximum_fusion.2), channel_id=1, source_target_pairs={{0,8},{8,16},{16,24},{24,32},{32,40},{40,48},{48,56},{56,64},{64,7... | collective-permute-start | bytes 12296 | tf_op jit(solution)/shard_map/ppermute | solution.py:63
Sparse Core Ops, SparseCore 0:
  10.4 101.8 all-gather.2
  115.3 88.5 all-gather.4
where the time goes:
time: 241 us; the launch traced here: 240 us
  waiting for transfers between devices  89 us (37%)
  blocking collectives  83.6 us (35%)
  matrix products  19.4 us (8%)
  local copies, waits for them, and re-layouts  15.3 us (6%)
  between operations  13.7 us (6%)
  other arithmetic  12.5 us (5%)
  starting transfers between devices  6.59 us (3%)
    all_gather x1, blocking collectives, in_one_piece(): whole = lax.all_gather(both, axis, axis=dim, tiled=True)  54.8 us
    all_gather x1, waiting for transfers between devices, rows_first(): whole = lax.all_gather(both, axis, axis=0, tiled=True)  45.6 us
    all_gather x1, waiting for transfers between devices, in_one_piece(): whole = lax.all_gather(both, axis, axis=dim, tiled=True)  38.8 us
    all_to_all x2, blocking collectives, sent_and_summed(): parts = lax.all_to_all(in_blocks(array, dim, size), axis, 0, 0, tiled=True)  28.8 us
    split x6, local copies, waits for them, and re-layouts, in_one_piece(): jnp.split(whole, [sum(widths[:k]) for k in range(1, len(widths))], axis=a...  13.6 us
    dot_general x2, matrix products, attend(): jnp.einsum('qhd,khd->qhk', queries, keys, preferred_element_type=jnp.floa...  7.16 us
    dot_general x2, matrix products, attend(): jnp.einsum('qhk,khd->qhd', weights.astype(jnp.bfloat16), values, preferre...  5.09 us
  transfers between devices with their start and end apart: 4, of which 3 were waited for; matrix products, arithmetic and copies ran while one was open for 16% of the time, Pallas kernels for 0%

commit v1 on v0

--- a/solution.py
+++ b/solution.py
@@ -11,7 +11,9 @@
     turned = [jnp.moveaxis(a, dim, 0) for a, dim in zip(arrays, dims)]
     widths = [t[0].size for t in turned]
     both = jnp.concatenate([t.reshape(-1, w) for t, w in zip(turned, widths)], axis=1)
-    whole = lax.all_gather(both, axis, axis=0, tiled=True)
+    whole = jnp.concatenate(
+        lax.all_to_all(jnp.stack([both] * lax.axis_size(axis)), axis, 0, 0), axis=0
+    )
     parts = jnp.split(whole, [sum(widths[:k]) for k in range(1, len(widths))], axis=1)
     return tuple(
         (

time: 241 us -> 429 us (1.78)
  the two profiles are of different devices: /device:TPU:64 before, /device:TPU:40 now
where the time goes in v1:
time: 429 us; the launch traced here: 428 us
  waiting for transfers between devices  263 us (61%)
  blocking collectives  67.6 us (16%)
  starting transfers between devices  27.4 us (6%)
  matrix products  23.8 us (6%)
  local copies, waits for them, and re-layouts  18.6 us (4%)
  between operations  13.7 us (3%)
  other arithmetic  13.5 us (3%)
    all_to_all x1, waiting for transfers between devices, rows_first(): lax.all_to_all(jnp.stack([both] * lax.axis_size(axis)), axis, 0, 0)  198 us
    all_gather x1, blocking collectives, in_one_piece(): whole = lax.all_gather(both, axis, axis=dim, tiled=True)  54.9 us
    all_gather x1, waiting for transfers between devices, in_one_piece(): whole = lax.all_gather(both, axis, axis=dim, tiled=True)  40.9 us
    all_to_all x1, blocking collectives, sent_and_summed(): parts = lax.all_to_all(in_blocks(array, dim, size), axis, 0, 0, tiled=True)  12.8 us
    split x6, local copies, waits for them, and re-layouts, in_one_piece(): jnp.split(whole, [sum(widths[:k]) for k in range(1, len(widths))], axis=a...  11.4 us
    dot_general x2, matrix products, attend(): jnp.einsum('qhd,khd->qhk', queries, keys, preferred_element_type=jnp.floa...  11 us
    all_to_all x1, starting transfers between devices, sent_to_all(): lax.all_to_all(jnp.broadcast_to(array[None], (size, *array.shape)), axis,...  10.9 us
    all_to_all x1, starting transfers between devices, rows_first(): lax.all_to_all(jnp.stack([both] * lax.axis_size(axis)), axis, 0, 0)  10.4 us
  transfers between devices with their start and end apart: 5, of which 5 were waited for; matrix products, arithmetic and copies ran while one was open for 2% of the time, Pallas kernels for 0%

profile of v1, /device:TPU:40, one launch (start us, length us, event | category | flops | bytes accessed | tf_op | source)
XLA Modules:
  0.0 427.8 jit_solution(12771863282821746170)
XLA Ops:
  6.5 1.5 pad_maximum_fusion
  10.2 54.9 %all_gather.7 = f32[8192,3]{0,1:T(4,128)S(1)} all-gather(f32[128,3]{0,1:T(4,128)S(1)} %pad_maximum_fusion.3), channel_id=1, replica_groups=mesh['sp'=64,'tp'=8] {'sp'}, dimensions={0}, use_global_device_ids=true | all-gather | bytes 99840 | tf_op jit(solution)/shard_map/all_gather | solution.py:29
  65.2 0.9 copy.43
  66.1 2.6 copy.48
  68.8 1.4 reduce-window_subtract_fusion.1
  71.2 1.7 iota_compare_fusion.1
  72.9 40.9 %all-gather.2.cloned.1.call-done = bf16[8192,512]{1,0:T(8,128)(2,1)} async-done(((bf16[128,512]{1,0:T(8,128)(2,1)}), bf16[8192,512]{1,0:T(8,128)(2,1)}) %all-gather.2.cloned.1.call-update) | async-done | bytes 8388624 | tf_op jit(solution)/shard_map/all_gather | solution.py:29
  113.7 4.2 fusion.74
  117.9 1.4 copy-done.3
  119.3 1.6 fusion.70
  120.9 4.1 copy.42
  125.0 3.4 fusion.16
  128.5 2.8 multiply_reduce_fusion.1
  131.2 3.0 copy.41
  134.2 6.8 %fusion.72 = (f32[128,2]{0,1:T(2,128)S(1)}, f32[128,2,8192]{0,2,1:T(8,128)S(1)}) fusion(f32[2,8192]{1,0:T(2,128)S(1)} %bitcast.93, f32[128,2]{0,1:T(2,128)S(1)} %constant_dynamic-slice_fusion.2, bf16[8192,2,64]{0,2,1:T(8,128)(2,1)} %bitcast.84, bf16[128,2,64]{0,2,1:T(8,128)(2,1)S(1)} %bitcast.95, pred[128,8192]{0,1:T(8,128)(4,1)} %iota_compare_fusion.1), kind=kOutput, calls=%fused_computation.97 | convolution fusion | flops 278920960 | bytes 11634688 | tf_op jit(solution)/shard_map/qhd,khd->qhk/dot_general | solution.py:84
  141.0 1.7 fusion.9
  142.7 2.1 multiply_reduce_fusion.2
  145.3 1.1 fusion.18
  146.4 4.3 all-to-all-start
  150.7 10.3 %all-to-all-done = bf16[8,16,2048]{2,1,0:T(8,128)(2,1)S(1)} async-done(((bf16[8,16,2048]{2,1,0:T(8,128)(2,1)}), bf16[8,16,2048]{2,1,0:T(8,128)(2,1)S(1)}, u32[]{:S(2)}, u32[]{:S(2)}) %all-to-all-start) | async-done | bytes 524320 | tf_op jit(solution)/shard_map/all_to_all | solution.py:40
  161.0 3.4 stack.2
  164.4 10.4 %all-to-all-start.2 = ((bf16[64,32,1536]{2,1,0:T(8,128)(2,1)}), bf16[64,32,1536]{2,1,0:T(8,128)(2,1)}, u32[]{:S(2)}, u32[]{:S(2)}) async-start(bf16[64,32,1536]{2,1,0:T(8,128)(2,1)} %stack.2), calls=%async_computation.2 | async-start | bytes 12582912 | tf_op jit(solution)/shard_map/all_to_all | solution.py:15
  175.1 198.1 %all-to-all-done.2 = bf16[64,32,1536]{2,1,0:T(8,128)(2,1)} async-done(((bf16[64,32,1536]{2,1,0:T(8,128)(2,1)}), bf16[64,32,1536]{2,1,0:T(8,128)(2,1)}, u32[]{:S(2)}, u32[]{:S(2)}) %all-to-all-start.2) | async-done | bytes 6291488 | tf_op jit(solution)/shard_map/all_to_all | solution.py:15
  373.2 0.9 broadcast_in_dim.63
  374.1 10.9 %all-to-all-start.1 = ((bf16[8,16,2048]{2,1,0:T(8,128)(2,1)}), bf16[8,16,2048]{2,1,0:T(8,128)(2,1)S(1)}, u32[]{:S(2)}, u32[]{:S(2)}) async-start(bf16[8,16,2048]{2,1,0:T(8,128)(2,1)} %broadcast_in_dim.63), calls=%async_computation.1 | async-start | bytes 1048576 | tf_op jit(solution)/shard_map/all_to_all | solution.py:46
  384.9 10.3 %all-to-all-done.1 = bf16[8,16,2048]{2,1,0:T(8,128)(2,1)S(1)} async-done(((bf16[8,16,2048]{2,1,0:T(8,128)(2,1)}), bf16[8,16,2048]{2,1,0:T(8,128)(2,1)S(1)}, u32[]{:S(2)}, u32[]{:S(2)}) %all-to-all-start.1) | async-done | bytes 524320 | tf_op jit(solution)/shard_map/all_to_all | solution.py:46
  395.2 2.0 fusion.35
  397.3 2.0 fusion.32
  399.3 1.9 collective-permute-start
  401.3 3.6 collective-permute-done
  405.1 2.4 convolution_convert_fusion
  407.5 12.8 %all_to_all.20 = bf16[8,16,2048]{2,1,0:T(8,128)(2,1)S(1)} all-to-all(bf16[8,16,2048]{2,1,0:T(8,128)(2,1)S(1)} %bitcast.88), channel_id=1, replica_groups=mesh['sp'=64,'tp'=8] {'tp'}, dimensions={0} | all-to-all | bytes 1048576 | tf_op jit(solution)/shard_map/all_to_all | solution.py:40
  (69 shorter events, 4.9 us)
Async XLA Ops:
  6.5 138.4 %copy-start = (bf16[128,2048]{1,0:T(8,128)(2,1)S(1)}, bf16[128,2048]{1,0:T(8,128)(2,1)}, u32[]{:S(2)}) copy-start(bf16[128,2048]{1,0:T(8,128)(2,1)} %param.26) | copy-start | bytes 1572868
  6.5 107.2 %copy-start.13 = (bf16[128,128]{1,0:T(8,128)(2,1)S(1)}, bf16[128,128]{1,0:T(8,128)(2,1)}, u32[]{:S(2)}) copy-start(bf16[128,128]{1,0:T(8,128)(2,1)} %param.21) | copy-start | bytes 98308
  6.5 107.2 %all-gather.2.cloned.1.call-start = ((), (), s32[]{:S(2)}) async-start(), calls=%async_computation.4 | async-start | bytes 8519680 | tf_op jit(solution)/shard_map/all_gather | solution.py:29
  113.7 5.6 %copy-start.3 = (bf16[8192,512]{1,0:T(8,128)(2,1)S(1)}, bf16[8192,512]{1,0:T(8,128)(2,1)}, u32[]{:S(2)}) copy-start(bf16[8192,512]{1,0:T(8,128)(2,1)} %all-gather.2.cloned.1.call-done) | copy-start | bytes 25165828
  125.0 3.4 copy-start.2
  134.2 6.8 %copy-start.1 = (pred[128,8192]{0,1:T(8,128)(4,1)S(1)}, pred[128,8192]{0,1:T(8,128)(4,1)}, u32[]{:S(2)}) copy-start(pred[128,8192]{0,1:T(8,128)(4,1)} %iota_compare_fusion.1) | copy-start | bytes 3145732
  141.0 1.7 copy-start.4
  142.7 2.6 copy-start.6
  144.9 5.8 %copy-start.7 = (bf16[512,32]{0,1:T(8,128)(2,1)S(1)}, bf16[512,32]{0,1:T(8,128)(2,1)}, u32[]{:S(2)}) copy-start(bf16[512,32]{0,1:T(8,128)(2,1)} %param.33) | copy-start | bytes 98308
  144.9 5.8 %copy-start.8 = (bf16[32,512]{1,0:T(8,128)(2,1)S(1)}, bf16[32,512]{1,0:T(8,128)(2,1)}, u32[]{:S(2)}) copy-start(bf16[32,512]{1,0:T(8,128)(2,1)} %param.30) | copy-start | bytes 98308
  144.9 5.8 %copy-start.9 = (bf16[32,512]{1,0:T(8,128)(2,1)S(1)}, bf16[32,512]{1,0:T(8,128)(2,1)}, u32[]{:S(2)}) copy-start(bf16[32,512]{1,0:T(8,128)(2,1)} %param.29) | copy-start | bytes 98308
  146.4 14.6 %all-to-all-start = ((bf16[8,16,2048]{2,1,0:T(8,128)(2,1)}), bf16[8,16,2048]{2,1,0:T(8,128)(2,1)S(1)}, u32[]{:S(2)}, u32[]{:S(2)}) async-start(bf16[8,16,2048]{2,1,0:T(8,128)(2,1)} %bitcast.20), calls=%async_computation | async-start | bytes 1048576 | tf_op jit(solution)/shard_map/all_to_all | solution.py:40
  164.4 10.5 %copy-start.5 = (bf16[16,2048]{1,0:T(8,128)(2,1)S(1)}, bf16[16,2048]{1,0:T(8,128)(2,1)}, u32[]{:S(2)}) copy-start(bf16[16,2048]{1,0:T(8,128)(2,1)} %param.17) | copy-start | bytes 196612
  164.4 10.6 %copy-start.10 = (f32[2048]{0:T(1024)S(1)}, f32[2048]{0:T(1024)}, u32[]{:S(2)}) copy-start(f32[2048]{0:T(1024)} %param.28) | copy-start | bytes 24580
  164.4 220.5 %copy-start.11 = (f32[3,512]{1,0:T(4,128)S(1)}, f32[3,512]{1,0:T(4,128)}, u32[]{:S(2)}) copy-start(f32[3,512]{1,0:T(4,128)} %param.31) | copy-start | bytes 18436
  164.4 220.5 %copy-start.12 = (f32[3,512]{1,0:T(4,128)S(1)}, f32[3,512]{1,0:T(4,128)}, u32[]{:S(2)}) copy-start(f32[3,512]{1,0:T(4,128)} %param.32) | copy-start | bytes 18436
  164.4 208.8 %all-to-all-start.2 = ((bf16[64,32,1536]{2,1,0:T(8,128)(2,1)}), bf16[64,32,1536]{2,1,0:T(8,128)(2,1)}, u32[]{:S(2)}, u32[]{:S(2)}) async-start(bf16[64,32,1536]{2,1,0:T(8,128)(2,1)} %stack.2), calls=%async_computation.2 | async-start | bytes 12582912 | tf_op jit(solution)/shard_map/all_to_all | solution.py:15
  374.1 21.2 %all-to-all-start.1 = ((bf16[8,16,2048]{2,1,0:T(8,128)(2,1)}), bf16[8,16,2048]{2,1,0:T(8,128)(2,1)S(1)}, u32[]{:S(2)}, u32[]{:S(2)}) async-start(bf16[8,16,2048]{2,1,0:T(8,128)(2,1)} %broadcast_in_dim.63), calls=%async_computation.1 | async-start | bytes 1048576 | tf_op jit(solution)/shard_map/all_to_all | solution.py:46
  399.3 5.5 %collective-permute-start = (bf16[2,1024]{1,0:T(2,128)(2,1)S(1)}, bf16[2,1024]{1,0:T(2,128)(2,1)S(1)}, u32[]{:S(2)}, u32[]{:S(2)}) collective-permute-start(bf16[2,1024]{1,0:T(2,128)(2,1)S(1)} %pad_maximum_fusion.2), channel_id=1, source_target_pairs={{0,8},{8,16},{16,24},{24,32},{32,40},{40,48},{48,56},{56,64},{64,7... | collective-permute-start | bytes 12296 | tf_op jit(solution)/shard_map/ppermute | solution.py:65
Sparse Core Ops, SparseCore 0:
  10.4 103.2 all-gather.1
